TPU v7x, 32 devices: a whole 2x2x4 slice. The times are simulated.
32 devices in a mesh: kv: 8 (over z, y), tp: 4 (over x, core).
Axes of the slice: x: 2, y: 2, z: 4, core: 2. Of those that a mesh axis runs over, the one named last changes fastest.
Arguments:
- tokens: bfloat16 [64, 6, 4096], P('kv'), may hold values from -6 to 6
- norm_gain: float32 [4096], replicated, may hold values from 0.1 to 1.9
- w_query: bfloat16 [4096, 2048], P('kv', 'tp'), may hold values from -0.09375 to 0.09375
- w_key: bfloat16 [4096, 2048], P('kv', 'tp'), may hold values from -0.09375 to 0.09375
- w_value: bfloat16 [4096, 2048], P('kv', 'tp'), may hold values from -0.09375 to 0.09375
- w_outgate: bfloat16 [4096, 2048], P('kv', 'tp'), may hold values from -0.09375 to 0.09375
- w_gates: bfloat16 [4096, 2, 16], P('kv', None, 'tp'), may hold values from -0.09375 to 0.09375
- forget_bias: float32 [16], P('tp'), may hold values from 1 to 6
- head_gain: float32 [2048], P('tp'), may hold values from 0.1 to 1.9
- w_mix: bfloat16 [2048, 4096], P('tp', 'kv'), may hold values from -0.125 to 0.125
- state_cell: float32 [64, 16, 128, 128], P('kv', 'tp'), may hold values from -4 to 4
- state_norm: float32 [64, 16, 128], P('kv', 'tp'), may hold values from -4 to 4
- state_max: float32 [64, 16], P('kv', 'tp'), may hold values from -4 to 120
- pend_keys: bfloat16 [64, 6, 2048], P('kv', None, 'tp'), may hold values from -6 to 6
- pend_values: bfloat16 [64, 6, 2048], P('kv', None, 'tp'), may hold values from -6 to 6
- pend_gates: float32 [64, 6, 2, 16], P('kv', None, None, 'tp'), may hold values from -6 to 6
- accepted: int32 [64], P('kv'), may hold values from 0 to 6
Outputs:
- mixed: bfloat16 [64, 6, 4096], P('kv', None, 'tp')
- new_cell: float32 [64, 16, 128, 128], P('kv', 'tp')
- new_norm: float32 [64, 16, 128], P('kv', 'tp')
- new_max: float32 [64, 16], P('kv', 'tp')
All inputs are finite; a program needn't handle non-finite values.
Results may differ from a plain program's by a relative error of at most 0.018.
Values may be sent and summed in bfloat16 or wider, within the bound.
A program may use at most 128 MiB of HBM per device.

v0:
```python
import jax
import jax.numpy as jnp
from jax import lax
from jax.sharding import PartitionSpec as P

epsilon = 1e-06
very_low = -1e30
highest = lax.Precision.HIGHEST


def shortened(shard):

    def short(part):
        return part.astype(jnp.bfloat16) if part.dtype == jnp.float32 else part

    return jax.tree.map(short, shard)


def from_partner(shard, axis, stride):
    return lax.ppermute(shard, axis, [(i, i ^ 1 << stride) for i in range(lax.axis_size(axis))])


def fold_pending(
    cell_state, normer, stabilizer, key_rows, value_rows, gate_rows, forget_shift, accepted
):
    proposals = key_rows.shape[1]
    accepted_mask = jnp.arange(proposals)[None, :, None] < accepted[:, None, None]
    log_in = jnp.where(accepted_mask, gate_rows[:, :, 0, :], very_low)
    log_keep = jnp.where(
        accepted_mask, jax.nn.log_sigmoid(gate_rows[:, :, 1, :] + forget_shift), 0.0
    )
    running = jnp.cumsum(log_keep, axis=1)
    block_total = running[:, -1]
    log_w = block_total[:, None, :] - running + log_in
    new_max = jnp.maximum(block_total + stabilizer, jnp.max(log_w, axis=1))
    weights = jnp.exp(log_w - new_max[:, None, :])
    carried = jnp.exp(block_total + stabilizer - new_max)
    weighted_keys = weights[..., None] * key_rows
    cell_new = carried[..., None, None] * cell_state + jnp.einsum(
        "sphd,sphe->shde", weighted_keys, value_rows, precision=highest
    )
    norm_new = carried[..., None] * normer + jnp.sum(weighted_keys, axis=1)
    return (cell_new, norm_new, new_max)


def read_block(queries, key_rows, value_rows, log_in, log_keep, cell_state, normer, stabilizer):
    proposals = queries.shape[1]
    causal = jnp.arange(proposals)[:, None] >= jnp.arange(proposals)[None, :]
    running_h = jnp.moveaxis(jnp.cumsum(log_keep, axis=1), 1, 2)
    input_h = jnp.moveaxis(log_in, 1, 2)
    log_d = jnp.where(
        causal, running_h[..., :, None] - running_h[..., None, :] + input_h[..., None, :], very_low
    )
    log_p = running_h + stabilizer[..., None]
    top_log = jnp.maximum(log_p, jnp.max(log_d, axis=-1))
    decays = jnp.exp(log_d - top_log[..., None])
    prior_w = jnp.exp(log_p - top_log)
    scores = jnp.einsum("sthd,suhd->shtu", queries, key_rows, precision=highest) * decays
    numerator = jnp.einsum("shtu,suhe->shte", scores, value_rows, precision=highest)
    numerator = numerator + prior_w[..., None] * jnp.einsum(
        "sthd,shde->shte", queries, cell_state, precision=highest
    )
    denominator = jnp.sum(scores, axis=-1) + prior_w * jnp.einsum(
        "sthd,shd->sht", queries, normer, precision=highest
    )
    hidden_out = numerator / jnp.maximum(jnp.abs(denominator), jnp.exp(-top_log))[..., None]
    return jnp.moveaxis(hidden_out, 1, 2)


def digit_of(own, bit):
    return own // 2**bit % 2


def collect_digits(pieces, dims, own, bits, sender):
    for bit in bits:
        others = sender(pieces, bit)
        first = digit_of(own, bit) == 0
        pieces = tuple(
            (
                jnp.where(
                    first,
                    jnp.concatenate((mine, theirs), axis=dim),
                    jnp.concatenate((theirs, mine), axis=dim),
                )
                for mine, theirs, dim in zip(pieces, others, dims)
            )
        )
    return pieces


def butterfly(blocks, own, near_bits, sender):
    for bit in range(near_bits):
        axis = near_bits - 1 - bit
        mine_digit = digit_of(own, bit)
        kept = lax.dynamic_index_in_dim(blocks, mine_digit, axis, keepdims=False)
        outgoing = lax.dynamic_index_in_dim(blocks, 1 - mine_digit, axis, keepdims=False)
        arrived = sender(outgoing, bit)
        blocks = jnp.where(
            mine_digit == 0,
            jnp.stack((kept, arrived), axis=axis),
            jnp.stack((arrived, kept), axis=axis),
        )
    return blocks


def halving(terms, own, near_bits, sender):
    for bit in range(near_bits - 1, -1, -1):
        mine_digit = digit_of(own, bit)
        kept = tuple(
            (lax.dynamic_index_in_dim(term, mine_digit, 0, keepdims=False) for term in terms)
        )
        outgoing = tuple(
            (lax.dynamic_index_in_dim(term, 1 - mine_digit, 0, keepdims=False) for term in terms)
        )
        arrived = sender(outgoing, bit)
        terms = tuple((left + right for left, right in zip(kept, arrived)))
    return terms


def shards(
    tokens,
    norm_gain,
    w_query,
    w_key,
    w_value,
    w_outgate,
    w_gates,
    forget_bias,
    head_gain,
    w_mix,
    state_cell,
    state_norm,
    state_max,
    pend_keys,
    pend_values,
    pend_gates,
    accepted,
):
    sequences, proposals, model_width = tokens.shape
    token_count = sequences * proposals
    local_heads = forget_bias.shape[0]
    head_size = state_cell.shape[-1]
    shard_rows = w_query.shape[0]
    flat_rows = tokens.reshape(token_count, model_width)
    own = lax.axis_index("kv")
    kv_bits = lax.axis_size("kv").bit_length() - 1
    near_bits = kv_bits // 2
    near = 2**near_bits
    far = lax.axis_size("kv") // near
    digit_shape = (2,) * near_bits
    collected = collect_digits(
        (w_query, w_key, w_value, w_outgate, w_gates.reshape(shard_rows, -1), w_mix),
        (0, 0, 0, 0, 0, 1),
        own,
        range(near_bits, kv_bits),
        lambda parts, bit: jax.tree.map(
            lambda part, own: part.astype(own.dtype),
            from_partner(shortened(parts), "kv", bit),
            parts,
        ),
    )
    far_mix = collected[5]
    token_digits = jnp.moveaxis(flat_rows.reshape(token_count, far, near, shard_rows), 2, 0)
    token_digits = token_digits.reshape(digit_shape + (token_count, far, shard_rows))
    arrived = butterfly(
        token_digits, own, near_bits, lambda part, bit: from_partner(part, "kv", bit)
    )
    gathered = arrived.reshape(near * token_count, far * shard_rows)
    gain_part = lax.dynamic_index_in_dim(
        norm_gain.reshape(far, near, shard_rows), own % near, 1, keepdims=False
    ).reshape(far * shard_rows)
    widened = gathered.astype(jnp.float32)
    scaled_in = (widened * gain_part).astype(jnp.bfloat16)
    partials = tuple(
        (
            jnp.dot(scaled_in, weight, preferred_element_type=jnp.float32).reshape(
                digit_shape + (token_count, weight.shape[1])
            )
            for weight in collected[:5]
        )
    )
    part_squares = jnp.sum(widened * widened, axis=-1).reshape(digit_shape + (token_count,))
    summed = halving(
        partials + (part_squares,),
        own,
        near_bits,
        lambda parts, bit: jax.tree.map(
            lambda part, own: part.astype(own.dtype),
            from_partner(shortened(parts), "kv", bit),
            parts,
        ),
    )
    totals = summed[:5]
    sum_squares = summed[5]
    row_scale = lax.rsqrt(sum_squares / model_width + epsilon)[:, None]
    queries = (totals[0] * row_scale).astype(jnp.bfloat16)
    new_keys = (totals[1] * row_scale).astype(jnp.bfloat16)
    new_values = (totals[2] * row_scale).astype(jnp.bfloat16)
    outgate = (totals[3] * row_scale).astype(jnp.bfloat16)
    gate_pre = (totals[4] * row_scale).reshape(sequences, proposals, 2, local_heads)

    def split_heads(array):
        return array.astype(jnp.float32).reshape(sequences, proposals, local_heads, head_size)

    key_scale = head_size ** (-0.5)
    cell_new, norm_new, new_max = fold_pending(
        state_cell,
        state_norm,
        state_max,
        split_heads(pend_keys) * key_scale,
        split_heads(pend_values),
        pend_gates,
        forget_bias,
        accepted,
    )
    log_in = gate_pre[:, :, 0, :]
    log_keep = jax.nn.log_sigmoid(gate_pre[:, :, 1, :] + forget_bias)
    hidden = read_block(
        split_heads(queries),
        split_heads(new_keys) * key_scale,
        split_heads(new_values),
        log_in,
        log_keep,
        cell_new,
        norm_new,
        new_max,
    )
    normed = hidden * lax.rsqrt(jnp.mean(hidden * hidden, axis=-1, keepdims=True) + epsilon)
    normed = normed * head_gain.reshape(local_heads, head_size)
    gated_rows = (jax.nn.sigmoid(split_heads(outgate)) * normed).astype(jnp.bfloat16)
    gated_rows = gated_rows.reshape(token_count, local_heads * head_size)
    near_gated = collect_digits(
        (gated_rows,),
        (0,),
        own,
        range(near_bits),
        lambda parts, bit: jax.tree.map(
            lambda part, own: part.astype(own.dtype),
            from_partner(shortened(parts), "kv", bit),
            parts,
        ),
    )[0]
    group_part = jnp.dot(near_gated, far_mix, preferred_element_type=jnp.float32).astype(
        jnp.bfloat16
    )
    group_part = group_part.reshape(digit_shape + (token_count, far, shard_rows))
    placed = butterfly(group_part, own, near_bits, lambda part, bit: from_partner(part, "kv", bit))
    placed = placed.reshape(near, token_count, far, shard_rows).transpose(1, 2, 0, 3)
    partial_out = placed.reshape(token_count, model_width).astype(jnp.float32)
    mixed_out = lax.psum_scatter(
        partial_out.astype(jnp.bfloat16), "tp", scatter_dimension=1, tiled=True
    )
    return (mixed_out.reshape(sequences, proposals, -1), cell_new, norm_new, new_max)


def solution(mesh):
    return jax.shard_map(
        shards,
        mesh=mesh,
        in_specs=(
            P("kv", None, None),
            P(),
            P("kv", "tp"),
            P("kv", "tp"),
            P("kv", "tp"),
            P("kv", "tp"),
            P("kv", None, "tp"),
            P("tp"),
            P("tp"),
            P("tp", "kv"),
            P("kv", "tp", None, None),
            P("kv", "tp", None),
            P("kv", "tp"),
            P("kv", None, "tp"),
            P("kv", None, "tp"),
            P("kv", None, None, "tp"),
            P("kv"),
        ),
        out_specs=(
            P("kv", None, "tp"),
            P("kv", "tp", None, None),
            P("kv", "tp", None),
            P("kv", "tp"),
        ),
        check_vma=False,
    )
```

profile of v0, /device:TPU:3, one launch (start us, length us, event | category | flops | bytes accessed | tf_op | source)
XLA Modules:
  0.0 338.9 jit_solution(17891725804589829772)
XLA Ops:
  10.6 1.8 fusion.90
  16.2 26.8 %collective-permute-done.11 = bf16[512,8]{0,1:T(8,128)(2,1)S(1)} collective-permute-done((bf16[512,8]{0,1:T(8,128)(2,1)S(1)}, bf16[512,8]{0,1:T(8,128)(2,1)S(1)}, u32[]{:S(2)}, u32[]{:S(2)}) %collective-permute-start.11) | collective-permute-done | bytes 8224 | tf_op jit(solution)/shard_map/ppermute | solution.py:20
  44.4 2.4 collective-permute-start.12
  47.3 7.5 %collective-permute-done.12 = bf16[1024,8]{0,1:T(8,128)(2,1)S(1)} collective-permute-done((bf16[1024,8]{0,1:T(8,128)(2,1)S(1)}, bf16[1024,8]{0,1:T(8,128)(2,1)S(1)}, u32[]{:S(2)}, u32[]{:S(2)}) %collective-permute-start.12) | collective-permute-done | bytes 16416 | tf_op jit(solution)/shard_map/ppermute | solution.py:20
  60.2 2.3 collective-permute-start.1
  62.8 1.6 reduce_window_sum.17
  67.3 1.6 maximum_select_fusion.9
  70.0 1.6 maximum_select_fusion.8
  71.6 2.3 collective-permute-start.9
  73.8 3.7 %multiply_add_fusion = f32[8,4,128,128]{3,2,1,0:T(8,128)S(1)} fusion(f32[8,4,128,128]{3,2,1,0:T(8,128)} %param.27, f32[8,4]{1,0:T(8,128)S(1)} %get-tuple-element.24, f32[8,6,4,128]{3,0,2,1:T(8,128)S(1)} %convert_bitcast_fusion, bf16[8,6,4,128]{3,0,2,1:T(8,128)(2,1)S(1)} %bitcast.161, f32[8,6,4]{1,2,0:T(4,128)S(1)} %exponential_multiply_fusion), kind=kOutput, calls=%fused_computation.15 | convolution fusion | flops 38821888 | bytes 4342656 | tf_op jit(solution)/shard_map/sphd,sphe->shde/dot_general | solution.py:39
  77.6 2.6 maximum_select_fusion.7
  80.4 1.8 maximum_select_fusion.6
  82.2 2.2 collective-permute-start.2
  84.5 97.6 %collective-permute-done.15 = bf16[1024,512]{1,0:T(8,128)(2,1)} collective-permute-done((bf16[1024,512]{1,0:T(8,128)(2,1)S(1)}, bf16[1024,512]{1,0:T(8,128)(2,1)}, u32[]{:S(2)}, u32[]{:S(2)}) %collective-permute-start.15) | collective-permute-done | bytes 1048608 | tf_op jit(solution)/shard_map/ppermute | solution.py:20
  182.1 2.3 fusion.9
  185.8 18.7 %collective-permute-done.9 = bf16[1024,512]{1,0:T(8,128)(2,1)S(1)} collective-permute-done((bf16[1024,512]{1,0:T(8,128)(2,1)S(1)}, bf16[1024,512]{1,0:T(8,128)(2,1)S(1)}, u32[]{:S(2)}, u32[]{:S(2)}) %collective-permute-start.9) | collective-permute-done | bytes 1048608 | tf_op jit(solution)/shard_map/ppermute | solution.py:20
  206.5 20.4 %collective-permute-done.6 = bf16[1024,512]{1,0:T(8,128)(2,1)S(1)} collective-permute-done((bf16[1024,512]{1,0:T(8,128)(2,1)S(1)}, bf16[1024,512]{1,0:T(8,128)(2,1)S(1)}, u32[]{:S(2)}, u32[]{:S(2)}) %collective-permute-start.6) | collective-permute-done | bytes 1048608 | tf_op jit(solution)/shard_map/ppermute | solution.py:20
  229.0 20.4 %collective-permute-done.2 = bf16[1024,512]{1,0:T(8,128)(2,1)S(1)} collective-permute-done((bf16[1024,512]{1,0:T(8,128)(2,1)S(1)}, bf16[1024,512]{1,0:T(8,128)(2,1)S(1)}, u32[]{:S(2)}, u32[]{:S(2)}) %collective-permute-start.2) | collective-permute-done | bytes 1048608 | tf_op jit(solution)/shard_map/ppermute | solution.py:20
  251.5 1.5 maximum_select_fusion.10
  255.0 1.8 fusion.93
  260.7 39.8 %collective-permute-done.19 = bf16[512,1024]{1,0:T(8,128)(2,1)} collective-permute-done((bf16[512,1024]{1,0:T(8,128)(2,1)S(1)}, bf16[512,1024]{1,0:T(8,128)(2,1)}, u32[]{:S(2)}, u32[]{:S(2)}) %collective-permute-start.19) | collective-permute-done | bytes 1048608 | tf_op jit(solution)/shard_map/ppermute | solution.py:20
  300.5 2.3 convolution_convert_fusion
  303.6 5.7 %collective-permute-done.20 = bf16[48,4,512]{2,0,1:T(8,128)(2,1)S(1)} collective-permute-done((bf16[48,4,512]{2,0,1:T(8,128)(2,1)S(1)}, bf16[48,4,512]{2,0,1:T(8,128)(2,1)S(1)}, u32[]{:S(2)}, u32[]{:S(2)}) %collective-permute-start.20) | collective-permute-done | bytes 196640 | tf_op jit(solution)/shard_map/ppermute | solution.py:20
  311.5 18.9 %reduce-scatter.2.cloned.1.call-done = bf16[48,1024]{1,0:T(8,128)(2,1)} async-done(((bf16[48,4096]{1,0:T(8,128)(2,1)}), bf16[48,1024]{1,0:T(8,128)(2,1)}) %reduce-scatter.2.cloned.1.call-update) | async-done | bytes 98320 | tf_op jit(solution)/shard_map/reduce_scatter | solution.py:250
  (151 shorter events, 36.5 us)
Async XLA Ops:
  7.2 323.2 %reduce-scatter.2.cloned.1.call-start = ((), (), s32[]{:S(2)}) async-start(), calls=%async_computation.1 | async-start | bytes 491520 | tf_op jit(solution)/shard_map/reduce_scatter | solution.py:250
  7.2 244.3 %collective-permute-start.18 = (bf16[512,512]{1,0:T(8,128)(2,1)}, bf16[512,512]{1,0:T(8,128)(2,1)}, u32[]{:S(2)}, u32[]{:S(2)}) collective-permute-start(bf16[512,512]{1,0:T(8,128)(2,1)} %param.26), channel_id=1, source_target_pairs={{0,8},{4,12},{8,0},{12,4},{16,24},{20,28},{24,16},{28,20},{1,9},{5... | collective-permute-start | bytes 1572872 | tf_op jit(solution)/shard_map/ppermute | solution.py:20
  8.6 58.7 %collective-permute-start.14 = (bf16[512,512]{1,0:T(8,128)(2,1)}, bf16[512,512]{1,0:T(8,128)(2,1)}, u32[]{:S(2)}, u32[]{:S(2)}) collective-permute-start(bf16[512,512]{1,0:T(8,128)(2,1)} %param.21), channel_id=1, source_target_pairs={{0,8},{4,12},{8,0},{12,4},{16,24},{20,28},{24,16},{28,20},{1,9},{5... | collective-permute-start | bytes 1572872 | tf_op jit(solution)/shard_map/ppermute | solution.py:20
  12.6 31.8 %collective-permute-start = (bf16[48,4,512]{2,0,1:T(8,128)(2,1)S(1)}, bf16[48,4,512]{2,0,1:T(8,128)(2,1)S(1)}, u32[]{:S(2)}, u32[]{:S(2)}) collective-permute-start(bf16[48,4,512]{2,0,1:T(8,128)(2,1)S(1)} %bitcast.168), channel_id=1, source_target_pairs={{0,4},{4,0},{8,12},{12,8},{16,20},{20,16},{24,28},{28,24},{1,5},{5... | collective-permute-start | bytes 589832 | tf_op jit(solution)/shard_map/ppermute | solution.py:20
  13.9 56.1 %collective-permute-start.8 = (bf16[512,512]{1,0:T(8,128)(2,1)S(1)}, bf16[512,512]{1,0:T(8,128)(2,1)}, u32[]{:S(2)}, u32[]{:S(2)}) collective-permute-start(bf16[512,512]{1,0:T(8,128)(2,1)S(1)} %copy-done.3), channel_id=1, source_target_pairs={{0,8},{4,12},{8,0},{12,4},{16,24},{20,28},{24,16},{28,20},{1,9},{5... | collective-permute-start | bytes 1572872 | tf_op jit(solution)/shard_map/ppermute | solution.py:20
  15.2 27.9 %collective-permute-start.11 = (bf16[512,8]{0,1:T(8,128)(2,1)S(1)}, bf16[512,8]{0,1:T(8,128)(2,1)S(1)}, u32[]{:S(2)}, u32[]{:S(2)}) collective-permute-start(bf16[512,8]{0,1:T(8,128)(2,1)S(1)} %reshape.216), channel_id=1, source_target_pairs={{0,8},{4,12},{8,0},{12,4},{16,24},{20,28},{24,16},{28,20},{1,9},{5... | collective-permute-start | bytes 24584 | tf_op jit(solution)/shard_map/ppermute | solution.py:20
  43.1 34.5 %collective-permute-start.5 = (bf16[512,512]{1,0:T(8,128)(2,1)}, bf16[512,512]{1,0:T(8,128)(2,1)}, u32[]{:S(2)}, u32[]{:S(2)}) collective-permute-start(bf16[512,512]{1,0:T(8,128)(2,1)} %param.19), channel_id=1, source_target_pairs={{0,8},{4,12},{8,0},{12,4},{16,24},{20,28},{24,16},{28,20},{1,9},{5... | collective-permute-start | bytes 1572872 | tf_op jit(solution)/shard_map/ppermute | solution.py:20
  44.4 10.4 %collective-permute-start.12 = (bf16[1024,8]{0,1:T(8,128)(2,1)S(1)}, bf16[1024,8]{0,1:T(8,128)(2,1)S(1)}, u32[]{:S(2)}, u32[]{:S(2)}) collective-permute-start(bf16[1024,8]{0,1:T(8,128)(2,1)S(1)} %maximum_select_fusion.17), channel_id=1, source_target_pairs={{0,16},{4,20},{8,24},{12,28},{16,0},{20,4},{24,8},{28,12},{1,17},{... | collective-permute-start | bytes 49160 | tf_op jit(solution)/shard_map/ppermute | solution.py:20
  54.8 2.8 collective-permute-start.4
  57.6 2.7 collective-permute-start.13
  60.2 20.2 %collective-permute-start.1 = (bf16[512,512]{1,0:T(8,128)(2,1)}, bf16[512,512]{1,0:T(8,128)(2,1)}, u32[]{:S(2)}, u32[]{:S(2)}) collective-permute-start(bf16[512,512]{1,0:T(8,128)(2,1)} %param.22), channel_id=1, source_target_pairs={{0,8},{4,12},{8,0},{12,4},{16,24},{20,28},{24,16},{28,20},{1,9},{5... | collective-permute-start | bytes 1572872 | tf_op jit(solution)/shard_map/ppermute | solution.py:20
  68.9 113.2 %collective-permute-start.15 = (bf16[1024,512]{1,0:T(8,128)(2,1)S(1)}, bf16[1024,512]{1,0:T(8,128)(2,1)}, u32[]{:S(2)}, u32[]{:S(2)}) collective-permute-start(bf16[1024,512]{1,0:T(8,128)(2,1)S(1)} %maximum_select_fusion.9), channel_id=1, source_target_pairs={{0,16},{4,20},{8,24},{12,28},{16,0},{20,4},{24,8},{28,12},{1,17},{... | collective-permute-start | bytes 3145736 | tf_op jit(solution)/shard_map/ppermute | solution.py:20
  71.6 132.9 %collective-permute-start.9 = (bf16[1024,512]{1,0:T(8,128)(2,1)S(1)}, bf16[1024,512]{1,0:T(8,128)(2,1)S(1)}, u32[]{:S(2)}, u32[]{:S(2)}) collective-permute-start(bf16[1024,512]{1,0:T(8,128)(2,1)S(1)} %maximum_select_fusion.8), channel_id=1, source_target_pairs={{0,16},{4,20},{8,24},{12,28},{16,0},{20,4},{24,8},{28,12},{1,17},{... | collective-permute-start | bytes 3145736 | tf_op jit(solution)/shard_map/ppermute | solution.py:20
  77.5 180.2 %copy-start.1 = (f32[8,4,128,128]{3,2,1,0:T(8,128)}, f32[8,4,128,128]{3,2,1,0:T(8,128)S(1)}, u32[]{:S(2)}) copy-start(f32[8,4,128,128]{3,2,1,0:T(8,128)S(1)} %multiply_add_fusion) | copy-start | bytes 6291460
  77.5 104.6 %copy-start.6 = (bf16[1,48,2048]{2,1,0:T(8,128)(2,1)S(1)}, bf16[1,48,2048]{2,1,0:T(8,128)(2,1)}, u32[]{:S(2)}) copy-start(bf16[1,48,2048]{2,1,0:T(8,128)(2,1)} %copy-done.5) | copy-start | bytes 589828
  80.2 146.8 %collective-permute-start.6 = (bf16[1024,512]{1,0:T(8,128)(2,1)S(1)}, bf16[1024,512]{1,0:T(8,128)(2,1)S(1)}, u32[]{:S(2)}, u32[]{:S(2)}) collective-permute-start(bf16[1024,512]{1,0:T(8,128)(2,1)S(1)} %maximum_select_fusion.7), channel_id=1, source_target_pairs={{0,16},{4,20},{8,24},{12,28},{16,0},{20,4},{24,8},{28,12},{1,17},{... | collective-permute-start | bytes 3145736 | tf_op jit(solution)/shard_map/ppermute | solution.py:20
  82.2 167.2 %collective-permute-start.2 = (bf16[1024,512]{1,0:T(8,128)(2,1)S(1)}, bf16[1024,512]{1,0:T(8,128)(2,1)S(1)}, u32[]{:S(2)}, u32[]{:S(2)}) collective-permute-start(bf16[1024,512]{1,0:T(8,128)(2,1)S(1)} %maximum_select_fusion.6), channel_id=1, source_target_pairs={{0,16},{4,20},{8,24},{12,28},{16,0},{20,4},{24,8},{28,12},{1,17},{... | collective-permute-start | bytes 3145736 | tf_op jit(solution)/shard_map/ppermute | solution.py:20
  184.5 68.6 %collective-permute-start.16 = (bf16[48,512]{1,0:T(8,128)(2,1)S(1)}, bf16[48,512]{1,0:T(8,128)(2,1)S(1)}, u32[]{:S(2)}, u32[]{:S(2)}) collective-permute-start(bf16[48,512]{1,0:T(8,128)(2,1)S(1)} %fusion.54), channel_id=1, source_target_pairs={{0,4},{4,0},{8,12},{12,8},{16,20},{20,16},{24,28},{28,24},{1,5},{5... | collective-permute-start | bytes 147464 | tf_op jit(solution)/shard_map/ppermute | solution.py:20
  205.2 47.9 %collective-permute-start.10 = (bf16[48,512]{1,0:T(8,128)(2,1)S(1)}, bf16[48,512]{1,0:T(8,128)(2,1)S(1)}, u32[]{:S(2)}, u32[]{:S(2)}) collective-permute-start(bf16[48,512]{1,0:T(8,128)(2,1)S(1)} %fusion.53), channel_id=1, source_target_pairs={{0,4},{4,0},{8,12},{12,8},{16,20},{20,16},{24,28},{28,24},{1,5},{5... | collective-permute-start | bytes 147464 | tf_op jit(solution)/shard_map/ppermute | solution.py:20
  227.7 25.4 %collective-permute-start.7 = (bf16[48,512]{1,0:T(8,128)(2,1)S(1)}, bf16[48,512]{1,0:T(8,128)(2,1)S(1)}, u32[]{:S(2)}, u32[]{:S(2)}) collective-permute-start(bf16[48,512]{1,0:T(8,128)(2,1)S(1)} %fusion.52), channel_id=1, source_target_pairs={{0,4},{4,0},{8,12},{12,8},{16,20},{20,16},{24,28},{28,24},{1,5},{5... | collective-permute-start | bytes 147464 | tf_op jit(solution)/shard_map/ppermute | solution.py:20
  250.2 3.0 collective-permute-start.3
  253.0 47.5 %collective-permute-start.19 = (bf16[512,1024]{1,0:T(8,128)(2,1)S(1)}, bf16[512,1024]{1,0:T(8,128)(2,1)}, u32[]{:S(2)}, u32[]{:S(2)}) collective-permute-start(bf16[512,1024]{1,0:T(8,128)(2,1)S(1)} %maximum_select_fusion.10), channel_id=1, source_target_pairs={{0,16},{4,20},{8,24},{12,28},{16,0},{20,4},{24,8},{28,12},{1,17},{... | collective-permute-start | bytes 3145736 | tf_op jit(solution)/shard_map/ppermute | solution.py:20
  259.4 41.1 %collective-permute-start.17 = (bf16[48,512]{1,0:T(8,128)(2,1)S(1)}, bf16[48,512]{1,0:T(8,128)(2,1)S(1)}, u32[]{:S(2)}, u32[]{:S(2)}) collective-permute-start(bf16[48,512]{1,0:T(8,128)(2,1)S(1)} %bitcast.170), channel_id=1, source_target_pairs={{0,4},{4,0},{8,12},{12,8},{16,20},{20,16},{24,28},{28,24},{1,5},{5... | collective-permute-start | bytes 147464 | tf_op jit(solution)/shard_map/ppermute | solution.py:20
  303.3 6.0 %collective-permute-start.20 = (bf16[48,4,512]{2,0,1:T(8,128)(2,1)S(1)}, bf16[48,4,512]{2,0,1:T(8,128)(2,1)S(1)}, u32[]{:S(2)}, u32[]{:S(2)}) collective-permute-start(bf16[48,4,512]{2,0,1:T(8,128)(2,1)S(1)} %bitcast.167), channel_id=1, source_target_pairs={{0,4},{4,0},{8,12},{12,8},{16,20},{20,16},{24,28},{28,24},{1,5},{5... | collective-permute-start | bytes 589832 | tf_op jit(solution)/shard_map/ppermute | solution.py:20
  (22 other events, 361.1 us)
Sparse Core Ops, SparseCore 0:
  311.0 19.3 reduce-scatter.1
where the time goes:
time: 342 us; the launch traced here: 339 us
  waiting for transfers between devices  259 us (76%)
  starting transfers between devices  24.7 us (7%)
  other arithmetic  15.5 us (5%)
  matrix products  15.2 us (4%)
  between operations  14.7 us (4%)
  local copies, waits for them, and re-layouts  10.3 us (3%)
    ppermute x21, waiting for transfers between devices, from_partner(): lax.ppermute(shard, axis, [(i, i ^ 1 << stride) for i in range(lax.axis_s...  240 us
    ppermute x21, starting transfers between devices, from_partner(): lax.ppermute(shard, axis, [(i, i ^ 1 << stride) for i in range(lax.axis_s...  24.7 us
    reduce_scatter x1, waiting for transfers between devices, shards(): lax.psum_scatter(partial_out.astype(jnp.bfloat16), 'tp', scatter_dimensio...  18.9 us
    select_n x6, other arithmetic, collect_digits(): jnp.where(first, jnp.concatenate((mine, theirs), axis=dim), jnp.concatena...  9.14 us
  transfers between devices with their start and end apart: 22, of which 12 were waited for; matrix products, arithmetic and copies ran while one was open for 10% of the time, Pallas kernels for 0%

commit v1 on v0

--- a/solution.py
+++ b/solution.py
@@ -1,6 +1,10 @@
+import functools
+
 import jax
 import jax.numpy as jnp
 from jax import lax
+from jax.experimental import pallas as pl
+from jax.experimental.pallas import tpu as pltpu
 from jax.sharding import PartitionSpec as P
 
 epsilon = 1e-06
@@ -115,6 +119,386 @@
         arrived = sender(outgoing, bit)
         terms = tuple((left + right for left, right in zip(kept, arrived)))
     return terms
+
+
+def greet(others):
+    barrier = pltpu.get_barrier_semaphore()
+    for where in others:
+        pl.semaphore_signal(
+            barrier, inc=1, device_id=where, device_id_type=pl.DeviceIdType.MESH
+        )
+    pl.semaphore_wait(barrier, len(others))
+
+
+def project_kernel(
+    ways,
+    tok_ref,
+    gain_ref,
+    wq_ref,
+    wk_ref,
+    wv_ref,
+    wo_ref,
+    wg_ref,
+    out_ref,
+    gate_ref,
+    tok_in,
+    wg_in,
+    part_out,
+    part_in,
+    total,
+    tok_send,
+    tok_recv,
+    wg_send,
+    wg_recv,
+    part_send,
+    part_recv,
+):
+    me = lax.axis_index("kv")
+    rows = wq_ref.shape[0]
+    width = wq_ref.shape[1]
+    model_width = tok_ref.shape[1]
+    greet([{"kv": lax.rem(me + step, ways)} for step in range(1, ways)])
+
+    def columns(owner):
+        return pl.ds(pl.multiple_of(owner * rows, rows), rows)
+
+    sends = []
+    for step in range(1, ways):
+        there = lax.rem(me + step, ways)
+        copy = pltpu.make_async_remote_copy(
+            src_ref=tok_ref.at[:, columns(there)],
+            dst_ref=tok_in.at[step],
+            send_sem=tok_send.at[step],
+            recv_sem=tok_recv.at[step],
+            device_id={"kv": there},
+            device_id_type=pl.DeviceIdType.MESH,
+        )
+        copy.start()
+        sends.append(copy)
+    gates_copies = []
+    for step in range(1, ways):
+        there = lax.rem(me + step, ways)
+        copy = pltpu.make_async_remote_copy(
+            src_ref=wg_ref,
+            dst_ref=wg_in.at[step],
+            send_sem=wg_send.at[step],
+            recv_sem=wg_recv.at[step],
+            device_id={"kv": there},
+            device_id_type=pl.DeviceIdType.MESH,
+        )
+        copy.start()
+        gates_copies.append(copy)
+
+    weights = (wq_ref, wk_ref, wv_ref, wo_ref)
+    gain = gain_ref[:, columns(me)]
+
+    def scaled(block, gain_part):
+        return (block.astype(jnp.float32) * gain_part).astype(jnp.bfloat16)
+
+    part_copies = []
+    for step in range(1, ways):
+        sends[step - 1].wait_recv()
+        block = scaled(tok_in[step], gain)
+        for index, weight in enumerate(weights):
+            part_out[step, :, index * width : (index + 1) * width] = jnp.dot(
+                block, weight[...], preferred_element_type=jnp.float32
+            ).astype(jnp.bfloat16)
+        back = lax.rem(me - step + ways, ways)
+        copy = pltpu.make_async_remote_copy(
+            src_ref=part_out.at[step],
+            dst_ref=part_in.at[step],
+            send_sem=part_send.at[step],
+            recv_sem=part_recv.at[step],
+            device_id={"kv": back},
+            device_id_type=pl.DeviceIdType.MESH,
+        )
+        copy.start()
+        part_copies.append(copy)
+
+    block = scaled(tok_ref[:, columns(me)], gain)
+    for index, weight in enumerate(weights):
+        total[:, index * width : (index + 1) * width] = jnp.dot(
+            block, weight[...], preferred_element_type=jnp.float32
+        )
+    contract = (((1,), (1,)), ((), ()))
+    gates = lax.dot_general(block, wg_ref[...], contract, preferred_element_type=jnp.float32)
+    squares = jnp.zeros((tok_ref.shape[0], 1), jnp.float32)
+    for step in range(ways):
+        part = tok_ref[:, step * rows : (step + 1) * rows].astype(jnp.float32)
+        squares = squares + jnp.sum(part * part, axis=1, keepdims=True)
+    row_scale = lax.rsqrt(squares / model_width + epsilon)
+    for step in range(1, ways):
+        gates_copies[step - 1].wait_recv()
+        owner = lax.rem(me - step + ways, ways)
+        block = scaled(tok_ref[:, columns(owner)], gain_ref[:, columns(owner)])
+        gates = gates + lax.dot_general(
+            block, wg_in[step], contract, preferred_element_type=jnp.float32
+        )
+    gate_ref[...] = gates * row_scale
+
+    for step in range(1, ways):
+        part_copies[step - 1].wait_recv()
+        for index in range(len(weights)):
+            place = slice(index * width, (index + 1) * width)
+            total[:, place] += part_in[step, :, place].astype(jnp.float32)
+    for index in range(len(weights)):
+        place = slice(index * width, (index + 1) * width)
+        out_ref[:, place] = (total[:, place] * row_scale).astype(jnp.bfloat16)
+    for copy in sends + gates_copies + part_copies:
+        copy.wait_send()
+
+
+def project(flat_rows, norm_gain, weights, w_gates):
+    ways = lax.axis_size("kv")
+    count, model_width = flat_rows.shape
+    rows, width = weights[0].shape
+    columns = width * len(weights)
+    gate_rows = w_gates.shape[1]
+    vmem = pl.BlockSpec(memory_space=pltpu.VMEM)
+    dma = pltpu.SemaphoreType.DMA((ways,))
+    return pl.pallas_call(
+        functools.partial(project_kernel, ways),
+        out_shape=(
+            jax.ShapeDtypeStruct((count, columns), jnp.bfloat16),
+            jax.ShapeDtypeStruct((count, gate_rows), jnp.float32),
+        ),
+        in_specs=[vmem] * 7,
+        out_specs=(vmem, vmem),
+        scratch_shapes=[
+            pltpu.VMEM((ways, count, rows), jnp.bfloat16),
+            pltpu.VMEM((ways, gate_rows, rows), jnp.bfloat16),
+            pltpu.VMEM((ways, count, columns), jnp.bfloat16),
+            pltpu.VMEM((ways, count, columns), jnp.bfloat16),
+            pltpu.VMEM((count, columns), jnp.float32),
+        ]
+        + [dma] * 6,
+        compiler_params=pltpu.CompilerParams(collective_id=0, has_side_effects=True),
+    )(flat_rows, norm_gain[None, :], *weights, w_gates.T)
+
+
+def mix_kernel(
+    ways,
+    groups,
+    gated_ref,
+    mix_ref,
+    out_ref,
+    gated_in,
+    part_out,
+    part_in,
+    gated_send,
+    gated_recv,
+    part_send,
+    part_recv,
+):
+    me = lax.axis_index("kv")
+    group = lax.axis_index("tp")
+    each = ways // groups
+    width = mix_ref.shape[1]
+    target = me // each
+    spot = lax.rem(me, each) * groups + group
+    at_home = target == group
+    barrier = pltpu.get_barrier_semaphore()
+
+    def signal(where):
+        pl.semaphore_signal(
+            barrier, inc=1, device_id=where, device_id_type=pl.DeviceIdType.MESH
+        )
+
+    for step in range(1, ways):
+        signal({"kv": lax.rem(me + step, ways)})
+    for which in range(each):
+        for other in range(groups):
+            sender = group * each + which
+
+            @pl.when(jnp.logical_or(sender != me, group != other))
+            def _():
+                signal({"kv": sender, "tp": other})
+
+    @pl.when(at_home)
+    def _():
+        pl.semaphore_wait(barrier, 2 * (ways - 1))
+
+    @pl.when(jnp.logical_not(at_home))
+    def _():
+        pl.semaphore_wait(barrier, 2 * (ways - 1) + 1)
+
+    gathers = []
+    for step in range(1, ways):
+        copy = pltpu.make_async_remote_copy(
+            src_ref=gated_ref,
+            dst_ref=gated_in.at[step],
+            send_sem=gated_send.at[step],
+            recv_sem=gated_recv.at[step],
+            device_id={"kv": lax.rem(me + step, ways)},
+            device_id_type=pl.DeviceIdType.MESH,
+        )
+        copy.start()
+        gathers.append(copy)
+
+    def outgoing(step, owner):
+        return pltpu.make_async_remote_copy(
+            src_ref=part_out.at[step],
+            dst_ref=part_in.at[spot],
+            send_sem=part_send.at[step],
+            recv_sem=part_recv.at[spot],
+            device_id={"kv": owner, "tp": target},
+            device_id_type=pl.DeviceIdType.MESH,
+        )
+
+    kept = pltpu.make_async_copy(part_out.at[0], part_in.at[spot], part_recv.at[spot])
+
+    def mixed(block):
+        return jnp.dot(block, mix_ref[...], preferred_element_type=jnp.float32).astype(
+            jnp.bfloat16
+        )
+
+    part_out[0] = mixed(gated_ref[...])
+
+    @pl.when(at_home)
+    def _():
+        kept.start()
+
+    @pl.when(jnp.logical_not(at_home))
+    def _():
+        outgoing(0, me).start()
+
+    copies = []
+    for step in range(1, ways):
+        gathers[step - 1].wait_recv()
+        part_out[step] = mixed(gated_in[step])
+        copy = outgoing(step, lax.rem(me - step + ways, ways))
+        copy.start()
+        copies.append(copy)
+
+    for which in range(each):
+        total = None
+        for other in range(groups):
+            slot = which * groups + other
+            pltpu.make_async_copy(part_out.at[0], part_in.at[slot], part_recv.at[slot]).wait()
+            term = part_in[slot].astype(jnp.float32)
+            total = term if total is None else total + term
+        out_ref[:, which * width : (which + 1) * width] = total.astype(jnp.bfloat16)
+    for copy in gathers + copies:
+        copy.wait_send()
+
+    @pl.when(jnp.logical_not(at_home))
+    def _():
+        outgoing(0, me).wait_send()
+
+
+def mix(gated_rows, w_mix):
+    ways, groups = lax.axis_size("kv"), lax.axis_size("tp")
+    count, rows = gated_rows.shape
+    width = w_mix.shape[1]
+    vmem = pl.BlockSpec(memory_space=pltpu.VMEM)
+    dma = pltpu.SemaphoreType.DMA((ways,))
+    return pl.pallas_call(
+        functools.partial(mix_kernel, ways, groups),
+        out_shape=jax.ShapeDtypeStruct((count, ways // groups * width), jnp.bfloat16),
+        in_specs=[vmem] * 2,
+        out_specs=vmem,
+        scratch_shapes=[
+            pltpu.VMEM((ways, count, rows), jnp.bfloat16),
+            pltpu.VMEM((ways, count, width), jnp.bfloat16),
+            pltpu.VMEM((ways, count, width), jnp.bfloat16),
+        ]
+        + [dma] * 4,
+        compiler_params=pltpu.CompilerParams(collective_id=1, has_side_effects=True),
+    )(gated_rows, w_mix)
+
+
+def project_by_digits(flat_rows, norm_gain, weights, w_mix):
+    token_count, model_width = flat_rows.shape
+    shard_rows = weights[0].shape[0]
+    own = lax.axis_index("kv")
+    kv_bits = lax.axis_size("kv").bit_length() - 1
+    near_bits = kv_bits // 2
+    near = 2**near_bits
+    far = lax.axis_size("kv") // near
+    digit_shape = (2,) * near_bits
+    collected = collect_digits(
+        weights + (w_mix,),
+        (0, 0, 0, 0, 0, 1),
+        own,
+        range(near_bits, kv_bits),
+        lambda parts, bit: jax.tree.map(
+            lambda part, own: part.astype(own.dtype),
+            from_partner(shortened(parts), "kv", bit),
+            parts,
+        ),
+    )
+    far_mix = collected[5]
+    token_digits = jnp.moveaxis(flat_rows.reshape(token_count, far, near, shard_rows), 2, 0)
+    token_digits = token_digits.reshape(digit_shape + (token_count, far, shard_rows))
+    arrived = butterfly(
+        token_digits, own, near_bits, lambda part, bit: from_partner(part, "kv", bit)
+    )
+    gathered = arrived.reshape(near * token_count, far * shard_rows)
+    gain_part = lax.dynamic_index_in_dim(
+        norm_gain.reshape(far, near, shard_rows), own % near, 1, keepdims=False
+    ).reshape(far * shard_rows)
+    widened = gathered.astype(jnp.float32)
+    scaled_in = (widened * gain_part).astype(jnp.bfloat16)
+    partials = tuple(
+        (
+            jnp.dot(scaled_in, weight, preferred_element_type=jnp.float32).reshape(
+                digit_shape + (token_count, weight.shape[1])
+            )
+            for weight in collected[:5]
+        )
+    )
+    part_squares = jnp.sum(widened * widened, axis=-1).reshape(digit_shape + (token_count,))
+    summed = halving(
+        partials + (part_squares,),
+        own,
+        near_bits,
+        lambda parts, bit: jax.tree.map(
+            lambda part, own: part.astype(own.dtype),
+            from_partner(shortened(parts), "kv", bit),
+            parts,
+        ),
+    )
+    totals = summed[:5]
+    sum_squares = summed[5]
+    row_scale = lax.rsqrt(sum_squares / model_width + epsilon)[:, None]
+    return (
+        tuple((total * row_scale).astype(jnp.bfloat16) for total in totals[:4]),
+        totals[4] * row_scale,
+        far_mix,
+    )
+
+
+def mix_by_digits(gated_rows, far_mix, model_width):
+    token_count = gated_rows.shape[0]
+    shard_rows = model_width // lax.axis_size("kv")
+    own = lax.axis_index("kv")
+    kv_bits = lax.axis_size("kv").bit_length() - 1
+    near_bits = kv_bits // 2
+    near = 2**near_bits
+    far = lax.axis_size("kv") // near
+    digit_shape = (2,) * near_bits
+    near_gated = collect_digits(
+        (gated_rows,),
+        (0,),
+        own,
+        range(near_bits),
+        lambda parts, bit: jax.tree.map(
+            lambda part, own: part.astype(own.dtype),
+            from_partner(shortened(parts), "kv", bit),
+            parts,
+        ),
+    )[0]
+    group_part = jnp.dot(near_gated, far_mix, preferred_element_type=jnp.float32).astype(
+        jnp.bfloat16
+    )
+    group_part = group_part.reshape(digit_shape + (token_count, far, shard_rows))
+    placed = butterfly(group_part, own, near_bits, lambda part, bit: from_partner(part, "kv", bit))
+    placed = placed.reshape(near, token_count, far, shard_rows).transpose(1, 2, 0, 3)
+    partial_out = placed.reshape(token_count, model_width).astype(jnp.float32)
+    mixed_out = lax.psum_scatter(
+        partial_out.astype(jnp.bfloat16), "tp", scatter_dimension=1, tiled=True
+    )
+    return mixed_out
 
 
 def shards(
@@ -141,63 +525,23 @@
     local_heads = forget_bias.shape[0]
     head_size = state_cell.shape[-1]
     shard_rows = w_query.shape[0]
+    weights = (w_query, w_key, w_value, w_outgate)
+    flat_gates = w_gates.reshape(shard_rows, -1)
     flat_rows = tokens.reshape(token_count, model_width)
-    own = lax.axis_index("kv")
-    kv_bits = lax.axis_size("kv").bit_length() - 1
-    near_bits = kv_bits // 2
-    near = 2**near_bits
-    far = lax.axis_size("kv") // near
-    digit_shape = (2,) * near_bits
-    collected = collect_digits(
-        (w_query, w_key, w_value, w_outgate, w_gates.reshape(shard_rows, -1), w_mix),
-        (0, 0, 0, 0, 0, 1),
-        own,
-        range(near_bits, kv_bits),
-        lambda parts, bit: jax.tree.map(
-            lambda part, own: part.astype(own.dtype),
-            from_partner(shortened(parts), "kv", bit),
-            parts,
-        ),
-    )
-    far_mix = collected[5]
-    token_digits = jnp.moveaxis(flat_rows.reshape(token_count, far, near, shard_rows), 2, 0)
-    token_digits = token_digits.reshape(digit_shape + (token_count, far, shard_rows))
-    arrived = butterfly(
-        token_digits, own, near_bits, lambda part, bit: from_partner(part, "kv", bit)
-    )
-    gathered = arrived.reshape(near * token_count, far * shard_rows)
-    gain_part = lax.dynamic_index_in_dim(
-        norm_gain.reshape(far, near, shard_rows), own % near, 1, keepdims=False
-    ).reshape(far * shard_rows)
-    widened = gathered.astype(jnp.float32)
-    scaled_in = (widened * gain_part).astype(jnp.bfloat16)
-    partials = tuple(
-        (
-            jnp.dot(scaled_in, weight, preferred_element_type=jnp.float32).reshape(
-                digit_shape + (token_count, weight.shape[1])
-            )
-            for weight in collected[:5]
-        )
-    )
-    part_squares = jnp.sum(widened * widened, axis=-1).reshape(digit_shape + (token_count,))
-    summed = halving(
-        partials + (part_squares,),
-        own,
-        near_bits,
-        lambda parts, bit: jax.tree.map(
-            lambda part, own: part.astype(own.dtype),
-            from_partner(shortened(parts), "kv", bit),
-            parts,
-        ),
-    )
-    totals = summed[:5]
-    sum_squares = summed[5]
-    row_scale = lax.rsqrt(sum_squares / model_width + epsilon)[:, None]
-    queries = (totals[0] * row_scale).astype(jnp.bfloat16)
-    new_keys = (totals[1] * row_scale).astype(jnp.bfloat16)
-    new_values = (totals[2] * row_scale).astype(jnp.bfloat16)
-    outgate = (totals[3] * row_scale).astype(jnp.bfloat16)
-    gate_pre = (totals[4] * row_scale).reshape(sequences, proposals, 2, local_heads)
+    direct = (
+        shard_rows % 128 == 0
+        and w_mix.shape[1] % 128 == 0
+        and lax.axis_size("kv") % lax.axis_size("tp") == 0
+    )
+    if direct:
+        columns, gate_pre = project(flat_rows, norm_gain, weights, flat_gates)
+        queries, new_keys, new_values, outgate = jnp.split(columns, len(weights), axis=1)
+    else:
+        projected, gate_pre, far_mix = project_by_digits(
+            flat_rows, norm_gain, weights + (flat_gates,), w_mix
+        )
+        queries, new_keys, new_values, outgate = projected
+    gate_pre = gate_pre.reshape(sequences, proposals, 2, local_heads)
 
     def split_heads(array):
         return array.astype(jnp.float32).reshape(sequences, proposals, local_heads, head_size)
@@ -229,27 +573,10 @@
     normed = normed * head_gain.reshape(local_heads, head_size)
     gated_rows = (jax.nn.sigmoid(split_heads(outgate)) * normed).astype(jnp.bfloat16)
     gated_rows = gated_rows.reshape(token_count, local_heads * head_size)
-    near_gated = collect_digits(
-        (gated_rows,),
-        (0,),
-        own,
-        range(near_bits),
-        lambda parts, bit: jax.tree.map(
-            lambda part, own: part.astype(own.dtype),
-            from_partner(shortened(parts), "kv", bit),
-            parts,
-        ),
-    )[0]
-    group_part = jnp.dot(near_gated, far_mix, preferred_element_type=jnp.float32).astype(
-        jnp.bfloat16
-    )
-    group_part = group_part.reshape(digit_shape + (token_count, far, shard_rows))
-    placed = butterfly(group_part, own, near_bits, lambda part, bit: from_partner(part, "kv", bit))
-    placed = placed.reshape(near, token_count, far, shard_rows).transpose(1, 2, 0, 3)
-    partial_out = placed.reshape(token_count, model_width).astype(jnp.float32)
-    mixed_out = lax.psum_scatter(
-        partial_out.astype(jnp.bfloat16), "tp", scatter_dimension=1, tiled=True
-    )
+    if direct:
+        mixed_out = mix(gated_rows, w_mix)
+    else:
+        mixed_out = mix_by_digits(gated_rows, far_mix, model_width)
     return (mixed_out.reshape(sequences, proposals, -1), cell_new, norm_new, new_max)
 
 

time: 342 us -> 102 us (0.30)
  waiting for transfers between devices: 259 us -> 0 us
  Pallas kernels: 0 us -> 77.4 us
  starting transfers between devices: 24.7 us -> 0 us
  between operations: 14.7 us -> 0.85 us
  matrix products: 15.2 us -> 5.73 us
  other arithmetic: 15.5 us -> 6.21 us
    ppermute x21 -> x0, waiting for transfers between devices: 240 us -> none  [from_partner(): lax.ppermute(shard, axis, [(i, i ^ 1 << stride) for i in range(lax.axis_s...]
    pallas_call x0 -> x2, Pallas kernels: none -> 77.4 us  [the longest x1 52.2 us: project(): pl.pallas_call(functools.partial(project_kernel, ways), out_shape=(jax.Sh...]
    ppermute x21 -> x0, starting transfers between devices: 24.7 us -> none  [from_partner(): lax.ppermute(shard, axis, [(i, i ^ 1 << stride) for i in range(lax.axis_s...]
    reduce_scatter x1 -> x0, waiting for transfers between devices: 18.9 us -> none  [shards(): lax.psum_scatter(partial_out.astype(jnp.bfloat16), 'tp', scatter_dimensio...]
    select_n x6 -> x0, other arithmetic: 9.14 us -> none  [collect_digits(): jnp.where(first, jnp.concatenate((mine, theirs), axis=dim), jnp.concatena...]
    dot_general x6 -> x0, matrix products: 7.18 us -> none  [the longest x5 4.87 us: shards(): jnp.dot(scaled_in, weight, preferred_element_type=jnp.float32)]
  transfers between devices with their start and end apart: 22 -> 0, of which waited for: 12 -> 0; matrix products, arithmetic and copies ran while one was open for 10% -> 0% of each run, Pallas kernels for 0% -> 0%
where the time goes in v1:
time: 102 us; the launch traced here: 101 us
  Pallas kernels  77.4 us (76%)
  local copies, waits for them, and re-layouts  11.1 us (11%)
  other arithmetic  6.21 us (6%)
  matrix products  5.73 us (6%)
    pallas_call x1, Pallas kernels, project(): pl.pallas_call(functools.partial(project_kernel, ways), out_shape=(jax.Sh...  52.2 us
    pallas_call x1, Pallas kernels, mix(): pl.pallas_call(functools.partial(mix_kernel, ways, groups), out_shape=jax...  25.2 us
    unnamed x22, local copies, waits for them, and re-layouts  5.11 us
    dot_general x1, matrix products, fold_pending(): jnp.einsum('sphd,sphe->shde', weighted_keys, value_rows, precision=highest)  3.7 us

profile of v1, /device:TPU:3, one launch (start us, length us, event | category | flops | bytes accessed | tf_op | source)
XLA Modules:
  0.0 101.2 jit_solution(9123605915464794331)
XLA Ops:
  0.6 0.8 copy-done
  1.4 0.7 iota_compare_fusion
  2.2 0.8 copy.128
  2.9 1.3 %reshape.104 = bf16[512,8]{0,1:T(8,128)(2,1)} reshape(bf16[512,2,4]{0,2,1:T(4,128)(2,1)} %param.23) | data formatting | bytes 16384 | tf_op jit(solution)/shard_map/reshape | solution.py:529
  4.2 0.7 fusion.26
  5.2 0.8 convert_bitcast_fusion
  6.0 1.2 %copy.118 = bf16[8,6,4096]{2,1,0:T(8,128)(2,1)S(1)} copy(bf16[8,6,4096]{2,0,1:T(8,128)(2,1)} %param.17) | data formatting | bytes 786432 | tf_op args[0]
  7.2 0.9 reshape.103.tok_ref
  8.1 52.2 %shard_map.192 = (bf16[48,2048]{1,0:T(8,128)(2,1)}, f32[48,8]{1,0:T(8,128)}) custom-call(bf16[48,4096]{1,0:T(8,128)(2,1)} %reshape.103.tok_ref, f32[1,4096]{1,0:T(1,128)} %bitcast.89, bf16[512,512]{1,0:T(8,128)(2,1)} %wq_ref.1, bf16[512,512]{1,0:T(8,128)(2,1)} %wk_ref.1, bf16[512,512]{1,0:T(8,128)(2,1)} %wv_ref.1, bf16[512,512]{1,0:T(8,128)(2,1)} %wo_ref.1, ...), custom_call_target="tpu_custom_call" | custom-call | tf_op jit(solution)/shard_map/pallas_call | solution.py:259
  60.3 0.8 copy.121
  61.4 1.4 %reduce_window_sum.17 = f32[8,6,4]{1,2,0:T(4,128)S(1)} reduce-window(f32[8,6,4]{1,2,0:T(4,128)S(1)} %get-tuple-element.40, f32[]{:T(128)} %constant.18.clone.1), window={size=1x6x1 pad=0_0x5_0x0_0}, to_apply=%region_0.1 | reduce-window | flops 960 | bytes 1540 | tf_op jit(solution)/shard_map/jit(cumsum)/reduce_window_sum | solution.py:53
  62.8 1.4 %reduce_window_sum.18 = f32[8,6,4]{1,2,0:T(4,128)S(1)} reduce-window(f32[8,6,4]{1,2,0:T(4,128)S(1)} %get-tuple-element.41, f32[]{:T(128)} %constant.18.clone.1), window={size=1x6x1 pad=0_0x5_0x0_0}, to_apply=%region_1.2 | reduce-window | flops 960 | bytes 1540 | tf_op jit(solution)/shard_map/jit(cumsum)/reduce_window_sum | solution.py:36
  64.7 0.7 copy.140
  65.9 0.8 fusion.24
  66.8 0.9 convert_multiply_fusion.1
  67.7 0.3 fusion.27
  68.0 0.2 fusion.8
  68.4 3.7 %multiply_add_fusion = f32[8,4,128,128]{3,2,1,0:T(8,128)S(1)} fusion(f32[8,4,128,128]{3,2,1,0:T(8,128)} %param.27, f32[8,4]{1,0:T(8,128)S(1)} %get-tuple-element.28, f32[8,6,4,128]{3,0,2,1:T(8,128)S(1)} %convert_bitcast_fusion, bf16[8,6,4,128]{3,0,2,1:T(8,128)(2,1)S(1)} %bitcast.81, f32[8,6,4]{1,2,0:T(4,128)S(1)} %exponential_multiply_fusion), kind=kOutput, calls=%fused_computation | convolution fusion | flops 38821888 | bytes 4342656 | tf_op jit(solution)/shard_map/sphd,sphe->shde/dot_general | solution.py:43
  72.1 1.1 %fusion.2 = f32[8,6,4,128]{3,1,2,0:T(8,128)S(1)} fusion(f32[8,4,128,128]{3,2,1,0:T(8,128)S(1)} %multiply_add_fusion, bf16[8,6,4,128]{3,2,1,0:T(4,128)(2,1)S(1)} %reshape.105, f32[8,6,4]{1,2,0:T(4,128)S(1)} %get-tuple-element.35), kind=kOutput, calls=%fused_computation.6 | convolution fusion | flops 37773312 | bytes 2245376 | tf_op jit(solution)/shard_map/sthd,shde->shte/dot_general | solution.py:64
  73.2 0.4 multiply_reduce_fusion
  73.8 0.6 copy.182
  74.4 25.2 %shard_map.193 = bf16[48,1024]{1,0:T(8,128)(2,1)} custom-call(bf16[48,512]{1,0:T(8,128)(2,1)} %bitcast.85, bf16[512,512]{1,0:T(8,128)(2,1)} %mix_ref.1), custom_call_target="tpu_custom_call" | custom-call | tf_op jit(solution)/shard_map/pallas_call | solution.py:395
  99.6 0.9 reshape.111
  100.5 0.7 copy.139
  (40 shorter events, 1.9 us)
Async XLA Ops:
  0.6 0.8 copy-start
  6.0 55.3 %copy-start.6 = (f32[4]{0:T(128)S(1)}, f32[4]{0:T(128)}, u32[]{:S(2)}) copy-start(f32[4]{0:T(128)} %param.24) | copy-start | bytes 52
  7.2 58.3 %copy-start.2 = (bf16[8,6,512]{2,0,1:T(8,128)(2,1)S(1)}, bf16[8,6,512]{2,0,1:T(8,128)(2,1)}, u32[]{:S(2)}) copy-start(bf16[8,6,512]{2,0,1:T(8,128)(2,1)} %param.30) | copy-start | bytes 147460
  7.2 58.4 %copy-start.3 = (f32[8,4,128]{2,1,0:T(4,128)S(1)}, f32[8,4,128]{2,1,0:T(4,128)}, u32[]{:S(2)}) copy-start(f32[8,4,128]{2,1,0:T(4,128)} %param.28) | copy-start | bytes 49156
  65.7 6.4 %copy-start.4 = (f32[8,4,128]{2,1,0:T(4,128)}, f32[8,4,128]{2,1,0:T(4,128)S(1)}, u32[]{:S(2)}) copy-start(f32[8,4,128]{2,1,0:T(4,128)S(1)} %multiply_add_fusion.1) | copy-start | bytes 49156
  72.1 27.5 %copy-start.1 = (f32[8,4,128,128]{3,2,1,0:T(8,128)}, f32[8,4,128,128]{3,2,1,0:T(8,128)S(1)}, u32[]{:S(2)}) copy-start(f32[8,4,128,128]{3,2,1,0:T(8,128)S(1)} %multiply_add_fusion) | copy-start | bytes 6291460
  72.1 1.5 %copy-start.5 = (f32[512]{0:T(512)S(1)}, f32[512]{0:T(512)}, u32[]{:S(2)}) copy-start(f32[512]{0:T(512)} %param.25) | copy-start | bytes 6148

commit v2 on v1

--- a/solution.py
+++ b/solution.py
@@ -22,6 +22,12 @@
 
 def from_partner(shard, axis, stride):
     return lax.ppermute(shard, axis, [(i, i ^ 1 << stride) for i in range(lax.axis_size(axis))])
+
+
+def running_sum(values):
+    steps = values.shape[1]
+    upto = jnp.arange(steps)[:, None] >= jnp.arange(steps)[None, :]
+    return jnp.sum(jnp.where(upto[None, :, :, None], values[:, None], 0.0), axis=2)
 
 
 def fold_pending(
@@ -33,7 +39,7 @@
     log_keep = jnp.where(
         accepted_mask, jax.nn.log_sigmoid(gate_rows[:, :, 1, :] + forget_shift), 0.0
     )
-    running = jnp.cumsum(log_keep, axis=1)
+    running = running_sum(log_keep)
     block_total = running[:, -1]
     log_w = block_total[:, None, :] - running + log_in
     new_max = jnp.maximum(block_total + stabilizer, jnp.max(log_w, axis=1))
@@ -50,7 +56,7 @@
 def read_block(queries, key_rows, value_rows, log_in, log_keep, cell_state, normer, stabilizer):
     proposals = queries.shape[1]
     causal = jnp.arange(proposals)[:, None] >= jnp.arange(proposals)[None, :]
-    running_h = jnp.moveaxis(jnp.cumsum(log_keep, axis=1), 1, 2)
+    running_h = jnp.moveaxis(running_sum(log_keep), 1, 2)
     input_h = jnp.moveaxis(log_in, 1, 2)
     log_d = jnp.where(
         causal, running_h[..., :, None] - running_h[..., None, :] + input_h[..., None, :], very_low
@@ -143,119 +149,157 @@
     gate_ref,
     tok_in,
     wg_in,
-    part_out,
-    part_in,
+    pair_out,
+    pair_in,
+    far_out,
+    far_in,
     total,
     tok_send,
     tok_recv,
     wg_send,
     wg_recv,
-    part_send,
-    part_recv,
+    pair_send,
+    pair_recv,
+    far_send,
+    far_recv,
 ):
     me = lax.axis_index("kv")
+    far = ways // 2
+    place, side = me // 2, lax.rem(me, 2)
     rows = wq_ref.shape[0]
     width = wq_ref.shape[1]
     model_width = tok_ref.shape[1]
-    greet([{"kv": lax.rem(me + step, ways)} for step in range(1, ways)])
+
+    def ahead(hop, other):
+        return 2 * lax.rem(place + hop, far) + (1 - side if other else side)
+
+    def behind(hop, other):
+        return 2 * lax.rem(place - hop + far, far) + (1 - side if other else side)
 
     def columns(owner):
         return pl.ds(pl.multiple_of(owner * rows, rows), rows)
 
-    sends = []
-    for step in range(1, ways):
-        there = lax.rem(me + step, ways)
+    def remote(source, target, send_sem, recv_sem, there):
         copy = pltpu.make_async_remote_copy(
-            src_ref=tok_ref.at[:, columns(there)],
-            dst_ref=tok_in.at[step],
-            send_sem=tok_send.at[step],
-            recv_sem=tok_recv.at[step],
+            src_ref=source,
+            dst_ref=target,
+            send_sem=send_sem,
+            recv_sem=recv_sem,
             device_id={"kv": there},
             device_id_type=pl.DeviceIdType.MESH,
         )
         copy.start()
-        sends.append(copy)
-    gates_copies = []
-    for step in range(1, ways):
-        there = lax.rem(me + step, ways)
-        copy = pltpu.make_async_remote_copy(
-            src_ref=wg_ref,
-            dst_ref=wg_in.at[step],
-            send_sem=wg_send.at[step],
-            recv_sem=wg_recv.at[step],
-            device_id={"kv": there},
-            device_id_type=pl.DeviceIdType.MESH,
-        )
-        copy.start()
-        gates_copies.append(copy)
+        return copy
+
+    hops = list(range(1, far))
+    peers = [(0, 1)] + [(hop, 1) for hop in hops] + [(hop, 0) for hop in hops]
+    greet([{"kv": ahead(hop, other)} for hop, other in peers])
+
+    tok_copies, wg_copies = {}, {}
+    for hop, other in peers:
+        slot = 2 * hop + other
+        there = ahead(hop, other)
+        tok_copies[slot] = remote(
+            tok_ref.at[:, columns(there)],
+            tok_in.at[slot],
+            tok_send.at[slot],
+            tok_recv.at[slot],
+            there,
+        )
+    for hop, other in peers:
+        slot = 2 * hop + other
+        wg_copies[slot] = remote(
+            wg_ref, wg_in.at[slot], wg_send.at[slot], wg_recv.at[slot], ahead(hop, other)
+        )
 
     weights = (wq_ref, wk_ref, wv_ref, wo_ref)
+    spans = [slice(index * width, (index + 1) * width) for index in range(len(weights))]
     gain = gain_ref[:, columns(me)]
 
     def scaled(block, gain_part):
         return (block.astype(jnp.float32) * gain_part).astype(jnp.bfloat16)
 
-    part_copies = []
-    for step in range(1, ways):
-        sends[step - 1].wait_recv()
-        block = scaled(tok_in[step], gain)
-        for index, weight in enumerate(weights):
-            part_out[step, :, index * width : (index + 1) * width] = jnp.dot(
-                block, weight[...], preferred_element_type=jnp.float32
-            ).astype(jnp.bfloat16)
-        back = lax.rem(me - step + ways, ways)
-        copy = pltpu.make_async_remote_copy(
-            src_ref=part_out.at[step],
-            dst_ref=part_in.at[step],
-            send_sem=part_send.at[step],
-            recv_sem=part_recv.at[step],
-            device_id={"kv": back},
-            device_id_type=pl.DeviceIdType.MESH,
-        )
-        copy.start()
-        part_copies.append(copy)
-
-    block = scaled(tok_ref[:, columns(me)], gain)
-    for index, weight in enumerate(weights):
-        total[:, index * width : (index + 1) * width] = jnp.dot(
-            block, weight[...], preferred_element_type=jnp.float32
-        )
-    contract = (((1,), (1,)), ((), ()))
-    gates = lax.dot_general(block, wg_ref[...], contract, preferred_element_type=jnp.float32)
+    def times(block, weight):
+        return jnp.dot(block, weight[...], preferred_element_type=jnp.float32)
+
+    pair_copies, far_copies = [], []
+    for hop in [0] + hops:
+        slot = 2 * hop + 1
+        tok_copies[slot].wait_recv()
+        block = scaled(tok_in[slot], gain)
+        for span, weight in zip(spans, weights):
+            pair_out[hop, :, span] = times(block, weight).astype(jnp.bfloat16)
+        pair_copies.append(
+            remote(
+                pair_out.at[hop],
+                pair_in.at[hop],
+                pair_send.at[hop],
+                pair_recv.at[hop],
+                behind(0, 1),
+            )
+        )
+
+    own_block = scaled(tok_ref[:, columns(me)], gain)
+    for span, weight in zip(spans, weights):
+        total[:, span] = times(own_block, weight)
     squares = jnp.zeros((tok_ref.shape[0], 1), jnp.float32)
     for step in range(ways):
         part = tok_ref[:, step * rows : (step + 1) * rows].astype(jnp.float32)
         squares = squares + jnp.sum(part * part, axis=1, keepdims=True)
     row_scale = lax.rsqrt(squares / model_width + epsilon)
-    for step in range(1, ways):
-        gates_copies[step - 1].wait_recv()
-        owner = lax.rem(me - step + ways, ways)
+
+    for hop in hops:
+        slot = 2 * hop
+        tok_copies[slot].wait_recv()
+        block = scaled(tok_in[slot], gain)
+        pair_copies[hop].wait_recv()
+        for span, weight in zip(spans, weights):
+            far_out[hop, :, span] = (
+                times(block, weight) + pair_in[hop, :, span].astype(jnp.float32)
+            ).astype(jnp.bfloat16)
+        far_copies.append(
+            remote(
+                far_out.at[hop],
+                far_in.at[hop],
+                far_send.at[hop],
+                far_recv.at[hop],
+                behind(hop, 0),
+            )
+        )
+
+    contract = (((1,), (1,)), ((), ()))
+    gates = lax.dot_general(own_block, wg_ref[...], contract, preferred_element_type=jnp.float32)
+    for hop, other in peers:
+        slot = 2 * hop + other
+        wg_copies[slot].wait_recv()
+        owner = behind(hop, other)
         block = scaled(tok_ref[:, columns(owner)], gain_ref[:, columns(owner)])
         gates = gates + lax.dot_general(
-            block, wg_in[step], contract, preferred_element_type=jnp.float32
+            block, wg_in[slot], contract, preferred_element_type=jnp.float32
         )
     gate_ref[...] = gates * row_scale
 
-    for step in range(1, ways):
-        part_copies[step - 1].wait_recv()
-        for index in range(len(weights)):
-            place = slice(index * width, (index + 1) * width)
-            total[:, place] += part_in[step, :, place].astype(jnp.float32)
-    for index in range(len(weights)):
-        place = slice(index * width, (index + 1) * width)
-        out_ref[:, place] = (total[:, place] * row_scale).astype(jnp.bfloat16)
-    for copy in sends + gates_copies + part_copies:
+    pair_copies[0].wait_recv()
+    for span in spans:
+        total[:, span] += pair_in[0, :, span].astype(jnp.float32)
+    for hop in hops:
+        far_copies[hop - 1].wait_recv()
+        for span in spans:
+            total[:, span] += far_in[hop, :, span].astype(jnp.float32)
+    for span in spans:
+        out_ref[:, span] = (total[:, span] * row_scale).astype(jnp.bfloat16)
+    for copy in list(tok_copies.values()) + list(wg_copies.values()) + pair_copies + far_copies:
         copy.wait_send()
 
 
 def project(flat_rows, norm_gain, weights, w_gates):
     ways = lax.axis_size("kv")
+    far = ways // 2
     count, model_width = flat_rows.shape
     rows, width = weights[0].shape
     columns = width * len(weights)
     gate_rows = w_gates.shape[1]
     vmem = pl.BlockSpec(memory_space=pltpu.VMEM)
-    dma = pltpu.SemaphoreType.DMA((ways,))
     return pl.pallas_call(
         functools.partial(project_kernel, ways),
         out_shape=(
@@ -267,11 +311,11 @@
         scratch_shapes=[
             pltpu.VMEM((ways, count, rows), jnp.bfloat16),
             pltpu.VMEM((ways, gate_rows, rows), jnp.bfloat16),
-            pltpu.VMEM((ways, count, columns), jnp.bfloat16),
-            pltpu.VMEM((ways, count, columns), jnp.bfloat16),
-            pltpu.VMEM((count, columns), jnp.float32),
         ]
-        + [dma] * 6,
+        + [pltpu.VMEM((far, count, columns), jnp.bfloat16)] * 4
+        + [pltpu.VMEM((count, columns), jnp.float32)]
+        + [pltpu.SemaphoreType.DMA((ways,))] * 4
+        + [pltpu.SemaphoreType.DMA((far,))] * 4,
         compiler_params=pltpu.CompilerParams(collective_id=0, has_side_effects=True),
     )(flat_rows, norm_gain[None, :], *weights, w_gates.T)
 
@@ -531,6 +575,7 @@
     direct = (
         shard_rows % 128 == 0
         and w_mix.shape[1] % 128 == 0
+        and lax.axis_size("kv") % 2 == 0
         and lax.axis_size("kv") % lax.axis_size("tp") == 0
     )
     if direct:

time: 102 us -> 87 us (0.85)
  Pallas kernels: 77.4 us -> 65.9 us
  other arithmetic: 6.21 us -> 3.09 us
    pallas_call x1, Pallas kernels: 52.2 us -> 36.2 us  [project(): pl.pallas_call(functools.partial(project_kernel, ways), out_shape=(jax.Sh...]
    pallas_call x1, Pallas kernels: 25.2 us -> 29.7 us  [mix(): pl.pallas_call(functools.partial(mix_kernel, ways, groups), out_shape=jax...]
    another operation x2 -> x0, other arithmetic: 2.81 us -> none  [the longest x1 1.41 us: read_block(): running_h = jnp.moveaxis(jnp.cumsum(log_keep, axis=1), 1, 2)]
    unnamed x22 -> x24, local copies, waits for them, and re-layouts: 5.11 us -> 4.34 us
where the time goes in v2:
time: 87 us; the launch traced here: 86.1 us
  Pallas kernels  65.9 us (76%)
  local copies, waits for them, and re-layouts  10.4 us (12%)
  matrix products  5.74 us (7%)
  other arithmetic  3.09 us (4%)
  between operations  0.88 us (1%)
    pallas_call x1, Pallas kernels, project(): pl.pallas_call(functools.partial(project_kernel, ways), out_shape=(jax.Sh...  36.2 us
    pallas_call x1, Pallas kernels, mix(): pl.pallas_call(functools.partial(mix_kernel, ways, groups), out_shape=jax...  29.7 us
    unnamed x24, local copies, waits for them, and re-layouts  4.34 us
    dot_general x1, matrix products, fold_pending(): jnp.einsum('sphd,sphe->shde', weighted_keys, value_rows, precision=highest)  3.7 us

profile of v2, /device:TPU:3, one launch (start us, length us, event | category | flops | bytes accessed | tf_op | source)
XLA Modules:
  0.0 86.1 jit_solution(7757882383493238470)
XLA Ops:
  0.6 0.8 copy-done
  1.4 0.7 iota_compare_fusion
  2.1 0.1 copy.159
  2.2 0.8 copy.168
  3.0 1.3 %reshape.148 = bf16[512,8]{0,1:T(8,128)(2,1)} reshape(bf16[512,2,4]{0,2,1:T(4,128)(2,1)} %param.23) | data formatting | bytes 16384 | tf_op jit(solution)/shard_map/reshape | solution.py:573
  4.3 0.8 convert_bitcast_fusion
  5.1 1.2 %copy.156 = bf16[8,6,4096]{2,1,0:T(8,128)(2,1)S(1)} copy(bf16[8,6,4096]{2,0,1:T(8,128)(2,1)} %param.17) | data formatting | bytes 786432 | tf_op args[0]
  6.4 0.9 %reshape.147.tok_ref = bf16[48,4096]{1,0:T(8,128)(2,1)} reshape(bf16[8,6,4096]{2,1,0:T(8,128)(2,1)S(1)} %copy.156) | data formatting | bytes 786432 | tf_op jit(solution)/shard_map/reshape | solution.py:574
  7.2 36.2 %shard_map.192 = (bf16[48,2048]{1,0:T(8,128)(2,1)}, f32[48,8]{1,0:T(8,128)}) custom-call(bf16[48,4096]{1,0:T(8,128)(2,1)} %reshape.147.tok_ref, f32[1,4096]{1,0:T(1,128)} %bitcast.93, bf16[512,512]{1,0:T(8,128)(2,1)} %wq_ref.1, bf16[512,512]{1,0:T(8,128)(2,1)} %wk_ref.1, bf16[512,512]{1,0:T(8,128)(2,1)} %wv_ref.1, bf16[512,512]{1,0:T(8,128)(2,1)} %wo_ref.1, ...), custom_call_target="tpu_custom_call" | custom-call | tf_op jit(solution)/shard_map/pallas_call | solution.py:303
  43.4 0.8 copy.160
  44.4 0.1 fusion.16
  44.6 0.1 select_reduce_fusion.1
  45.1 0.2 fusion.5
  45.8 0.8 fusion.24
  46.7 0.9 %convert_multiply_fusion.1 = (f32[48,512]{1,0:T(8,128)S(1)}, f32[48,512]{1,0:T(8,128)S(1)}) fusion(bf16[48,2048]{1,0:T(8,128)(2,1)} %get-tuple-element.6), kind=kLoop, calls=%fused_computation.17 | loop fusion | flops 147456 | bytes 294912 | tf_op jit(solution)/shard_map/mul | solution.py:609
  47.6 0.3 fusion.26
  48.0 0.3 fusion.8
  48.6 3.7 %multiply_add_fusion = f32[8,4,128,128]{3,2,1,0:T(8,128)S(1)} fusion(f32[8,4,128,128]{3,2,1,0:T(8,128)} %param.27, f32[8,4]{1,0:T(8,128)S(1)} %get-tuple-element.34, f32[8,6,4,128]{3,0,2,1:T(8,128)S(1)} %convert_bitcast_fusion, bf16[8,6,4,128]{3,0,2,1:T(8,128)(2,1)S(1)} %bitcast.86, f32[8,6,4]{1,2,0:T(4,128)S(1)} %copy.179), kind=kOutput, calls=%fused_computation | convolution fusion | flops 38821888 | bytes 4342656 | tf_op jit(solution)/shard_map/sphd,sphe->shde/dot_general | solution.py:49
  52.4 1.1 %fusion.2 = f32[8,6,4,128]{3,1,2,0:T(8,128)S(1)} fusion(f32[8,4,128,128]{3,2,1,0:T(8,128)S(1)} %multiply_add_fusion, bf16[8,6,4,128]{3,2,1,0:T(4,128)(2,1)S(1)} %reshape.149, f32[8,6,4]{1,2,0:T(4,128)S(1)} %copy.178), kind=kOutput, calls=%fused_computation.6 | convolution fusion | flops 37773312 | bytes 2245376 | tf_op jit(solution)/shard_map/sthd,shde->shte/dot_general | solution.py:70
  53.4 0.4 multiply_reduce_fusion
  54.0 0.6 copy.225
  54.7 29.7 %shard_map.193 = bf16[48,1024]{1,0:T(8,128)(2,1)} custom-call(bf16[48,512]{1,0:T(8,128)(2,1)} %bitcast.89, bf16[512,512]{1,0:T(8,128)(2,1)} %mix_ref.1), custom_call_target="tpu_custom_call" | custom-call | tf_op jit(solution)/shard_map/pallas_call | solution.py:439
  84.4 0.9 %reshape.155 = bf16[8,6,1024]{2,1,0:T(8,128)(2,1)S(1)} reshape(bf16[48,1024]{1,0:T(8,128)(2,1)} %shard_map.193) | data formatting | bytes 196608 | tf_op jit(solution)/shard_map/reshape | solution.py:625
  85.4 0.7 copy.188
  (49 shorter events, 1.8 us)
Async XLA Ops:
  0.6 0.8 copy-start
  5.1 39.3 %copy-start.3 = (f32[8,6,2,4]{0,3,2,1:T(4,128)S(1)}, f32[8,6,2,4]{0,3,2,1:T(4,128)}, u32[]{:S(2)}) copy-start(f32[8,6,2,4]{0,3,2,1:T(4,128)} %param.32) | copy-start | bytes 4612
  5.1 39.3 %copy-start.8 = (f32[4]{0:T(128)S(1)}, f32[4]{0:T(128)}, u32[]{:S(2)}) copy-start(f32[4]{0:T(128)} %param.24) | copy-start | bytes 52
  6.3 39.2 %copy-start.2 = (bf16[8,6,512]{2,0,1:T(8,128)(2,1)S(1)}, bf16[8,6,512]{2,0,1:T(8,128)(2,1)}, u32[]{:S(2)}) copy-start(bf16[8,6,512]{2,0,1:T(8,128)(2,1)} %param.30) | copy-start | bytes 147460
  6.3 39.3 %copy-start.5 = (f32[8,4,128]{2,1,0:T(4,128)S(1)}, f32[8,4,128]{2,1,0:T(4,128)}, u32[]{:S(2)}) copy-start(f32[8,4,128]{2,1,0:T(4,128)} %param.28) | copy-start | bytes 49156
  45.0 7.4 %copy-start.4 = (f32[8,4]{0,1:T(4,128)}, f32[8,4]{0,1:T(4,128)S(1)}, u32[]{:S(2)}) copy-start(f32[8,4]{0,1:T(4,128)S(1)} %copy.171) | copy-start | bytes 388
  45.7 6.7 %copy-start.6 = (f32[8,4,128]{2,1,0:T(4,128)}, f32[8,4,128]{2,1,0:T(4,128)S(1)}, u32[]{:S(2)}) copy-start(f32[8,4,128]{2,1,0:T(4,128)S(1)} %multiply_add_fusion.1) | copy-start | bytes 49156
  52.4 32.1 %copy-start.1 = (f32[8,4,128,128]{3,2,1,0:T(8,128)}, f32[8,4,128,128]{3,2,1,0:T(8,128)S(1)}, u32[]{:S(2)}) copy-start(f32[8,4,128,128]{3,2,1,0:T(8,128)S(1)} %multiply_add_fusion) | copy-start | bytes 6291460
  52.4 1.5 %copy-start.7 = (f32[512]{0:T(512)S(1)}, f32[512]{0:T(512)}, u32[]{:S(2)}) copy-start(f32[512]{0:T(512)} %param.25) | copy-start | bytes 6148

commit v3 on v2

--- a/solution.py
+++ b/solution.py
@@ -192,7 +192,7 @@
         return copy
 
     hops = list(range(1, far))
-    peers = [(0, 1)] + [(hop, 1) for hop in hops] + [(hop, 0) for hop in hops]
+    peers = [(hop, 1) for hop in hops] + [(0, 1)] + [(hop, 0) for hop in hops]
     greet([{"kv": ahead(hop, other)} for hop, other in peers])
 
     tok_copies, wg_copies = {}, {}
@@ -222,22 +222,22 @@
     def times(block, weight):
         return jnp.dot(block, weight[...], preferred_element_type=jnp.float32)
 
-    pair_copies, far_copies = [], []
-    for hop in [0] + hops:
+    halves = (slice(0, 2 * width), slice(2 * width, 4 * width))
+    pair_copies, far_copies = {}, {}
+    for hop in hops + [0]:
         slot = 2 * hop + 1
         tok_copies[slot].wait_recv()
         block = scaled(tok_in[slot], gain)
-        for span, weight in zip(spans, weights):
-            pair_out[hop, :, span] = times(block, weight).astype(jnp.bfloat16)
-        pair_copies.append(
-            remote(
-                pair_out.at[hop],
-                pair_in.at[hop],
-                pair_send.at[hop],
-                pair_recv.at[hop],
+        for half, cut in enumerate(halves):
+            for index in (2 * half, 2 * half + 1):
+                pair_out[hop, :, spans[index]] = times(block, weights[index]).astype(jnp.bfloat16)
+            pair_copies[hop, half] = remote(
+                pair_out.at[hop, :, cut],
+                pair_in.at[hop, :, cut],
+                pair_send.at[2 * hop + half],
+                pair_recv.at[2 * hop + half],
                 behind(0, 1),
             )
-        )
 
     own_block = scaled(tok_ref[:, columns(me)], gain)
     for span, weight in zip(spans, weights):
@@ -252,20 +252,20 @@
         slot = 2 * hop
         tok_copies[slot].wait_recv()
         block = scaled(tok_in[slot], gain)
-        pair_copies[hop].wait_recv()
-        for span, weight in zip(spans, weights):
-            far_out[hop, :, span] = (
-                times(block, weight) + pair_in[hop, :, span].astype(jnp.float32)
-            ).astype(jnp.bfloat16)
-        far_copies.append(
-            remote(
-                far_out.at[hop],
-                far_in.at[hop],
-                far_send.at[hop],
-                far_recv.at[hop],
+        for half, cut in enumerate(halves):
+            pair_copies[hop, half].wait_recv()
+            for index in (2 * half, 2 * half + 1):
+                span = spans[index]
+                far_out[hop, :, span] = (
+                    times(block, weights[index]) + pair_in[hop, :, span].astype(jnp.float32)
+                ).astype(jnp.bfloat16)
+            far_copies[hop, half] = remote(
+                far_out.at[hop, :, cut],
+                far_in.at[hop, :, cut],
+                far_send.at[2 * hop + half],
+                far_recv.at[2 * hop + half],
                 behind(hop, 0),
             )
-        )
 
     contract = (((1,), (1,)), ((), ()))
     gates = lax.dot_general(own_block, wg_ref[...], contract, preferred_element_type=jnp.float32)
@@ -279,17 +279,20 @@
         )
     gate_ref[...] = gates * row_scale
 
-    pair_copies[0].wait_recv()
+    pair_copies[0, 0].wait_recv()
+    pair_copies[0, 1].wait_recv()
     for span in spans:
         total[:, span] += pair_in[0, :, span].astype(jnp.float32)
     for hop in hops:
-        far_copies[hop - 1].wait_recv()
+        far_copies[hop, 0].wait_recv()
+        far_copies[hop, 1].wait_recv()
         for span in spans:
             total[:, span] += far_in[hop, :, span].astype(jnp.float32)
     for span in spans:
         out_ref[:, span] = (total[:, span] * row_scale).astype(jnp.bfloat16)
-    for copy in list(tok_copies.values()) + list(wg_copies.values()) + pair_copies + far_copies:
-        copy.wait_send()
+    for group in (tok_copies, wg_copies, pair_copies, far_copies):
+        for copy in group.values():
+            copy.wait_send()
 
 
 def project(flat_rows, norm_gain, weights, w_gates):
@@ -314,8 +317,7 @@
         ]
         + [pltpu.VMEM((far, count, columns), jnp.bfloat16)] * 4
         + [pltpu.VMEM((count, columns), jnp.float32)]
-        + [pltpu.SemaphoreType.DMA((ways,))] * 4
-        + [pltpu.SemaphoreType.DMA((far,))] * 4,
+        + [pltpu.SemaphoreType.DMA((ways,))] * 8,
         compiler_params=pltpu.CompilerParams(collective_id=0, has_side_effects=True),
     )(flat_rows, norm_gain[None, :], *weights, w_gates.T)
 
@@ -366,18 +368,27 @@
     def _():
         pl.semaphore_wait(barrier, 2 * (ways - 1) + 1)
 
-    gathers = []
-    for step in range(1, ways):
+    far = ways // 2
+    place, side = me // 2, lax.rem(me, 2)
+    partner = 2 * place + 1 - side
+    hops = list(range(1, far))
+
+    def gather(source, slot, there):
         copy = pltpu.make_async_remote_copy(
-            src_ref=gated_ref,
-            dst_ref=gated_in.at[step],
-            send_sem=gated_send.at[step],
-            recv_sem=gated_recv.at[step],
-            device_id={"kv": lax.rem(me + step, ways)},
+            src_ref=source,
+            dst_ref=gated_in.at[slot],
+            send_sem=gated_send.at[slot],
+            recv_sem=gated_recv.at[slot],
+            device_id={"kv": there},
             device_id_type=pl.DeviceIdType.MESH,
         )
         copy.start()
-        gathers.append(copy)
+        return copy
+
+    gathers = {}
+    for hop in hops:
+        gathers[2 * hop] = gather(gated_ref, 2 * hop, 2 * lax.rem(place + hop, far) + side)
+    gathers[1] = gather(gated_ref, 1, partner)
 
     def outgoing(step, owner):
         return pltpu.make_async_remote_copy(
@@ -407,12 +418,22 @@
         outgoing(0, me).start()
 
     copies = []
-    for step in range(1, ways):
-        gathers[step - 1].wait_recv()
-        part_out[step] = mixed(gated_in[step])
-        copy = outgoing(step, lax.rem(me - step + ways, ways))
+
+    def answer(slot, owner):
+        part_out[slot] = mixed(gated_in[slot])
+        copy = outgoing(slot, owner)
         copy.start()
         copies.append(copy)
+
+    for hop in hops:
+        slot = 2 * hop
+        gathers[slot].wait_recv()
+        gathers[slot + 1] = gather(gated_in.at[slot], slot + 1, partner)
+        answer(slot, 2 * lax.rem(place - hop + far, far) + side)
+    for hop in [0] + hops:
+        slot = 2 * hop + 1
+        gathers[slot].wait_recv()
+        answer(slot, 2 * lax.rem(place - hop + far, far) + 1 - side)
 
     for which in range(each):
         total = None
@@ -422,7 +443,7 @@
             term = part_in[slot].astype(jnp.float32)
             total = term if total is None else total + term
         out_ref[:, which * width : (which + 1) * width] = total.astype(jnp.bfloat16)
-    for copy in gathers + copies:
+    for copy in list(gathers.values()) + copies:
         copy.wait_send()
 
     @pl.when(jnp.logical_not(at_home))

time: 87 us -> 76.9 us (0.88)
  Pallas kernels: 65.9 us -> 55.4 us
    pallas_call x1, Pallas kernels: 29.7 us -> 22.5 us  [mix(): pl.pallas_call(functools.partial(mix_kernel, ways, groups), out_shape=jax...]
    pallas_call x1, Pallas kernels: 36.2 us -> 32.8 us  [project(): pl.pallas_call(functools.partial(project_kernel, ways), out_shape=(jax.Sh...]
where the time goes in v3:
time: 76.9 us; the launch traced here: 75.5 us
  Pallas kernels  55.4 us (72%)
  local copies, waits for them, and re-layouts  10.4 us (14%)
  matrix products  5.73 us (7%)
  other arithmetic  3.09 us (4%)
  between operations  0.88 us (1%)
    pallas_call x1, Pallas kernels, project(): pl.pallas_call(functools.partial(project_kernel, ways), out_shape=(jax.Sh...  32.8 us
    pallas_call x1, Pallas kernels, mix(): pl.pallas_call(functools.partial(mix_kernel, ways, groups), out_shape=jax...  22.5 us
    unnamed x24, local copies, waits for them, and re-layouts  4.34 us
    dot_general x1, matrix products, fold_pending(): jnp.einsum('sphd,sphe->shde', weighted_keys, value_rows, precision=highest)  3.7 us

profile of v3, /device:TPU:3, one launch (start us, length us, event | category | flops | bytes accessed | tf_op | source)
XLA Modules:
  0.0 75.5 jit_solution(18045197387965039850)
XLA Ops:
  0.6 0.8 %copy-done = bf16[8,6,512]{2,0,1:T(8,128)(2,1)S(1)} copy-done((bf16[8,6,512]{2,0,1:T(8,128)(2,1)S(1)}, bf16[8,6,512]{2,0,1:T(8,128)(2,1)}, u32[]{:S(2)}) %copy-start) | copy-done | bytes 49176
  1.4 0.7 iota_compare_fusion
  2.1 0.1 copy.159
  2.2 0.8 %copy.168 = f32[8,4]{1,0:T(8,128)S(1)} copy(f32[8,4]{0,1:T(4,128)} %param.29) | data formatting | bytes 256 | tf_op args[12]
  3.0 1.3 %reshape.148 = bf16[512,8]{0,1:T(8,128)(2,1)} reshape(bf16[512,2,4]{0,2,1:T(4,128)(2,1)} %param.23) | data formatting | bytes 16384 | tf_op jit(solution)/shard_map/reshape | solution.py:594
  4.3 0.8 %convert_bitcast_fusion = f32[8,6,4,128]{3,0,2,1:T(8,128)S(1)} fusion(bf16[8,6,512]{2,0,1:T(8,128)(2,1)} %param.30), kind=kLoop, calls=%fused_computation.15 | loop fusion | flops 24576 | bytes 147456 | tf_op jit(solution)/shard_map/reshape | solution.py:613
  5.1 1.2 %copy.156 = bf16[8,6,4096]{2,1,0:T(8,128)(2,1)S(1)} copy(bf16[8,6,4096]{2,0,1:T(8,128)(2,1)} %param.17) | data formatting | bytes 786432 | tf_op args[0]
  6.4 0.9 %reshape.147.tok_ref = bf16[48,4096]{1,0:T(8,128)(2,1)} reshape(bf16[8,6,4096]{2,1,0:T(8,128)(2,1)S(1)} %copy.156) | data formatting | bytes 786432 | tf_op jit(solution)/shard_map/reshape | solution.py:595
  7.2 32.8 %shard_map.192 = (bf16[48,2048]{1,0:T(8,128)(2,1)}, f32[48,8]{1,0:T(8,128)}) custom-call(bf16[48,4096]{1,0:T(8,128)(2,1)} %reshape.147.tok_ref, f32[1,4096]{1,0:T(1,128)} %bitcast.93, bf16[512,512]{1,0:T(8,128)(2,1)} %wq_ref.1, bf16[512,512]{1,0:T(8,128)(2,1)} %wk_ref.1, bf16[512,512]{1,0:T(8,128)(2,1)} %wv_ref.1, bf16[512,512]{1,0:T(8,128)(2,1)} %wo_ref.1, ...), custom_call_target="tpu_custom_call" | custom-call | tf_op jit(solution)/shard_map/pallas_call | solution.py:306
  40.1 0.8 %copy.160 = f32[48,8]{0,1:T(8,128)S(1)} copy(f32[48,8]{1,0:T(8,128)} %get-tuple-element.7) | data formatting | bytes 3072 | tf_op jit(solution)/shard_map/pallas_call | solution.py:306
  41.1 0.1 fusion.16
  41.2 0.1 select_reduce_fusion.1
  41.8 0.2 fusion.5
  42.5 0.8 %fusion.24 = (bf16[48,512]{1,0:T(8,128)(2,1)S(1)}, bf16[48,512]{1,0:T(8,128)(2,1)S(1)}) fusion(bf16[48,2048]{1,0:T(8,128)(2,1)} %get-tuple-element.6), kind=kLoop, calls=%fused_computation.56 | loop fusion | bytes 196608 | tf_op jit(solution)/shard_map/split | solution.py:604
  43.3 0.9 %convert_multiply_fusion.1 = (f32[48,512]{1,0:T(8,128)S(1)}, f32[48,512]{1,0:T(8,128)S(1)}) fusion(bf16[48,2048]{1,0:T(8,128)(2,1)} %get-tuple-element.6), kind=kLoop, calls=%fused_computation.17 | loop fusion | flops 147456 | bytes 294912 | tf_op jit(solution)/shard_map/mul | solution.py:630
  44.2 0.3 fusion.26
  44.6 0.2 fusion.8
  45.3 3.7 %multiply_add_fusion = f32[8,4,128,128]{3,2,1,0:T(8,128)S(1)} fusion(f32[8,4,128,128]{3,2,1,0:T(8,128)} %param.27, f32[8,4]{1,0:T(8,128)S(1)} %get-tuple-element.34, f32[8,6,4,128]{3,0,2,1:T(8,128)S(1)} %convert_bitcast_fusion, bf16[8,6,4,128]{3,0,2,1:T(8,128)(2,1)S(1)} %bitcast.86, f32[8,6,4]{1,2,0:T(4,128)S(1)} %copy.179), kind=kOutput, calls=%fused_computation | convolution fusion | flops 38821888 | bytes 4342656 | tf_op jit(solution)/shard_map/sphd,sphe->shde/dot_general | solution.py:49
  49.0 1.1 %fusion.2 = f32[8,6,4,128]{3,1,2,0:T(8,128)S(1)} fusion(f32[8,4,128,128]{3,2,1,0:T(8,128)S(1)} %multiply_add_fusion, bf16[8,6,4,128]{3,2,1,0:T(4,128)(2,1)S(1)} %reshape.149, f32[8,6,4]{1,2,0:T(4,128)S(1)} %copy.178), kind=kOutput, calls=%fused_computation.6 | convolution fusion | flops 37773312 | bytes 2245376 | tf_op jit(solution)/shard_map/sthd,shde->shte/dot_general | solution.py:70
  50.1 0.4 multiply_reduce_fusion
  50.7 0.6 copy.225
  51.3 22.5 %shard_map.193 = bf16[48,1024]{1,0:T(8,128)(2,1)} custom-call(bf16[48,512]{1,0:T(8,128)(2,1)} %bitcast.89, bf16[512,512]{1,0:T(8,128)(2,1)} %mix_ref.1), custom_call_target="tpu_custom_call" | custom-call | tf_op jit(solution)/shard_map/pallas_call | solution.py:460
  73.9 0.9 %reshape.155 = bf16[8,6,1024]{2,1,0:T(8,128)(2,1)S(1)} reshape(bf16[48,1024]{1,0:T(8,128)(2,1)} %shard_map.193) | data formatting | bytes 196608 | tf_op jit(solution)/shard_map/reshape | solution.py:646
  74.8 0.7 copy.188
  (49 shorter events, 1.8 us)
Async XLA Ops:
  0.6 0.8 %copy-start = (bf16[8,6,512]{2,0,1:T(8,128)(2,1)S(1)}, bf16[8,6,512]{2,0,1:T(8,128)(2,1)}, u32[]{:S(2)}) copy-start(bf16[8,6,512]{2,0,1:T(8,128)(2,1)} %param.31) | copy-start | bytes 147460
  5.1 36.0 %copy-start.3 = (f32[8,6,2,4]{0,3,2,1:T(4,128)S(1)}, f32[8,6,2,4]{0,3,2,1:T(4,128)}, u32[]{:S(2)}) copy-start(f32[8,6,2,4]{0,3,2,1:T(4,128)} %param.32) | copy-start | bytes 4612
  5.1 36.0 %copy-start.8 = (f32[4]{0:T(128)S(1)}, f32[4]{0:T(128)}, u32[]{:S(2)}) copy-start(f32[4]{0:T(128)} %param.24) | copy-start | bytes 52
  6.3 35.8 %copy-start.2 = (bf16[8,6,512]{2,0,1:T(8,128)(2,1)S(1)}, bf16[8,6,512]{2,0,1:T(8,128)(2,1)}, u32[]{:S(2)}) copy-start(bf16[8,6,512]{2,0,1:T(8,128)(2,1)} %param.30) | copy-start | bytes 147460
  6.3 35.9 %copy-start.5 = (f32[8,4,128]{2,1,0:T(4,128)S(1)}, f32[8,4,128]{2,1,0:T(4,128)}, u32[]{:S(2)}) copy-start(f32[8,4,128]{2,1,0:T(4,128)} %param.28) | copy-start | bytes 49156
  41.6 7.4 %copy-start.4 = (f32[8,4]{0,1:T(4,128)}, f32[8,4]{0,1:T(4,128)S(1)}, u32[]{:S(2)}) copy-start(f32[8,4]{0,1:T(4,128)S(1)} %copy.171) | copy-start | bytes 388
  42.3 6.6 %copy-start.6 = (f32[8,4,128]{2,1,0:T(4,128)}, f32[8,4,128]{2,1,0:T(4,128)S(1)}, u32[]{:S(2)}) copy-start(f32[8,4,128]{2,1,0:T(4,128)S(1)} %multiply_add_fusion.1) | copy-start | bytes 49156
  49.0 24.8 %copy-start.1 = (f32[8,4,128,128]{3,2,1,0:T(8,128)}, f32[8,4,128,128]{3,2,1,0:T(8,128)S(1)}, u32[]{:S(2)}) copy-start(f32[8,4,128,128]{3,2,1,0:T(8,128)S(1)} %multiply_add_fusion) | copy-start | bytes 6291460
  49.0 1.5 %copy-start.7 = (f32[512]{0:T(512)S(1)}, f32[512]{0:T(512)}, u32[]{:S(2)}) copy-start(f32[512]{0:T(512)} %param.25) | copy-start | bytes 6148
